TPU v7x, 32 devices: a whole 2x2x4 slice. The times are simulated.
32 devices in a mesh: sp: 8 (over z, x), tp: 4 (over y, core).
Axes of the slice: x: 2, y: 2, z: 4, core: 2. Of those that a mesh axis runs over, the one named last changes fastest.
Arguments:
- queries: bfloat16 [2048, 1024], P('sp', 'tp'), may hold values from -64 to 64
- keys: bfloat16 [2048, 1024], P('sp', 'tp'), may hold values from -64 to 64
- values: bfloat16 [2048, 1024], P('sp', 'tp'), may hold values from -6 to 6
- cum_gate: float32 [16, 2048], P('tp'), may hold values from -2048 to 0, as said below
- out_weight: bfloat16 [1024, 2048], P('tp'), may hold values from -0.375 to 0.375
- resid: bfloat16 [2048, 2048], P('sp'), may hold values from -6 to 6
- norm_gain: float32 [2048], replicated, may hold values from 0.1 to 1.9
- routes: int32 [2048, 2], P('sp'), may hold values from 0 to 7, all different within a row; in each aligned block of 256 rows (0 to 255, 256 to 511, ...) at most 80 rows name the same one
- route_weight: float32 [2048, 2], P('sp'), may hold values from 0.1 to 0.9
- gate_weight: bfloat16 [8, 2048, 4096], P('sp', None, 'tp'), may hold values from -0.125 to 0.125
- up_weight: bfloat16 [8, 2048, 4096], P('sp', None, 'tp'), may hold values from -0.125 to 0.125
- down_weight: bfloat16 [8, 4096, 2048], P('sp', 'tp'), may hold values from -0.09375 to 0.09375
Outputs:
- layer_out: bfloat16 [2048, 2048], P('sp', 'tp')
Inputs may be any that keep to these rules, and one draw needn't show every extreme that they name: `routes`: each token names 2 different experts. Among the rows of one index of sp, no expert is named more than 80 times, a bound that some block reaches. `cum_gate`: each head's row does not rise along the positions.
All inputs are finite; a program needn't handle non-finite values.
Results may differ from a plain program's by a relative error of at most 0.015.
Values may be sent and summed in bfloat16 or wider, within the bound.
A program may use at most 64 MiB of HBM per device.

v0:
```python
import functools

import jax
import jax.numpy as jnp
from jax import lax
from jax.experimental import pallas as pl
from jax.experimental.pallas import tpu as pltpu
from jax.sharding import PartitionSpec as P

HD = 64
LANES = 128
EPSILON = 1e-06
MESH = pl.DeviceIdType.MESH
VMEM_BYTES = 60 * 1024 * 1024


def remote(src, dst, send_sem, recv_sem, s, t):
    return pltpu.make_async_remote_copy(
        src_ref=src,
        dst_ref=dst,
        send_sem=send_sem,
        recv_sem=recv_sem,
        device_id=(s, t),
        device_id_type=MESH,
    )


def offset_of(d, sp):
    half = sp // 2
    low, top = (d // 2) % 2, d // half
    return d - 2 * low - half * top + half * low + 2 * top


def greet(sp, tp, s, t):
    barrier = pltpu.get_barrier_semaphore()
    for d in range(1, sp):
        pl.semaphore_signal(barrier, inc=1, device_id=(s ^ d, t), device_id_type=MESH)
    for a in range(1, tp):
        pl.semaphore_signal(barrier, inc=1, device_id=(s, t ^ a), device_id_type=MESH)
    pl.semaphore_wait(barrier, sp + tp - 2)


class Gather:
    def __init__(self, buf, y_send, p_send, recv, s, t, tp):
        self.buf, self.y_send, self.p_send, self.recv = buf, y_send, p_send, recv
        self.s, self.t, self.ny = s, t, tp // 2

    def y_copy(self, k):
        at = self.buf.at[self.t]
        return remote(at, at, self.y_send.at[k], self.recv.at[self.t], self.s, self.t ^ (2 * k))

    def p_copy(self, k):
        a = self.t ^ (2 * k)
        at = self.buf.at[a]
        return remote(at, at, self.p_send.at[k], self.recv.at[a], self.s, self.t ^ 1)

    def arrival(self, a):
        at = self.buf.at[a]
        return remote(at, at, self.p_send.at[0], self.recv.at[a], self.s, self.t ^ 1)

    def start(self):
        for k in range(1, self.ny):
            self.y_copy(k).start()
        self.p_copy(0).start()

    def relay(self):
        for k in range(1, self.ny):
            self.arrival(self.t ^ (2 * k)).wait_recv()
            self.p_copy(k).start()

    def finish(self):
        for k in range(self.ny):
            self.arrival(self.t ^ (2 * k + 1)).wait_recv()

    def drain(self):
        for k in range(1, self.ny):
            self.y_copy(k).wait_send()
        for k in range(self.ny):
            self.p_copy(k).wait_send()


def attend_kernel(
    sp, tp, hpd, q_ref, kv_ref, cq_ref, ck_ref, w_ref, resid_ref, gain_ref, pick_ref,
    stream_out, rows_out,
    qbuf, kvbuf, osend, obuf, wbuf, attbuf, stream, normed,
    q_send, q_recv, kv_send, kv_recv, o_send, o_recv, local_sem,
    wy_send, wp_send, w_recv, ay_send, ap_send, a_recv,
):
    s, t = lax.axis_index("sp"), lax.axis_index("tp")
    g = sp // hpd
    piece = q_ref.shape[1]
    rows = kv_ref.shape[1]
    cols = stream_out.shape[1]
    own_w = pltpu.make_async_copy(w_ref, wbuf.at[t], local_sem.at[0])
    own_w.start()
    own_q = pltpu.make_async_copy(q_ref.at[s], qbuf.at[s], local_sem.at[1])
    own_q.start()
    own_kv = pltpu.make_async_copy(kv_ref.at[s // g], kvbuf.at[s], local_sem.at[2])
    own_kv.start()
    greet(sp, tp, s, t)

    def q_copy(d):
        dst = s ^ d
        return remote(q_ref.at[dst], qbuf.at[s], q_send.at[d], q_recv.at[s], dst, t)

    def kv_copy(d):
        dst = s ^ d
        return remote(kv_ref.at[dst // g], kvbuf.at[s], kv_send.at[d], kv_recv.at[s], dst, t)

    for d in range(sp - 1, 0, -1):
        kv_copy(d).start()
        q_copy(d).start()
    own_w.wait()
    w_gather = Gather(wbuf, wy_send, wp_send, w_recv, s, t, tp)
    w_gather.start()
    own_q.wait()
    own_kv.wait()
    first = lax.rem(s, g) * piece

    def o_copy(i):
        return remote(osend.at[i], obuf.at[s], o_send.at[i], o_recv.at[s], i, t)

    for i in range(sp):
        @pl.when(s != i)
        def _():
            remote(qbuf.at[i], qbuf.at[i], q_send.at[0], q_recv.at[i], s ^ 1, t).wait_recv()
            remote(kvbuf.at[i], kvbuf.at[i], kv_send.at[0], kv_recv.at[i], s ^ 1, t).wait_recv()

        q = qbuf[i]
        cq = cq_ref[i]
        kv_here = kvbuf[i]
        contract = (((1,), (1,)), ((), ()))
        diag = lax.dot_general(q, kv_here, contract, preferred_element_type=jnp.float32)
        diag = diag + cq - ck_ref[:, i * rows:(i + 1) * rows]
        qpos = first + lax.broadcasted_iota(jnp.int32, diag.shape, 0)
        kpos = lax.broadcasted_iota(jnp.int32, diag.shape, 1)
        diag = jnp.where(kpos <= qpos, diag, -jnp.inf)
        best = jnp.max(diag, axis=1, keepdims=True)
        if i:
            kv_past = kvbuf[0:i].reshape(i * rows, LANES)
            past = lax.dot_general(q, kv_past, contract, preferred_element_type=jnp.float32)
            past = past + cq - ck_ref[:, :i * rows]
            best = jnp.maximum(best, jnp.max(past, axis=1, keepdims=True))
        weights = jnp.exp(diag - best)
        total = jnp.sum(weights, axis=1, keepdims=True)
        value = jnp.dot(weights.astype(jnp.bfloat16), kv_here, preferred_element_type=jnp.float32)
        if i:
            weights = jnp.exp(past - best)
            total = total + jnp.sum(weights, axis=1, keepdims=True)
            value = value + jnp.dot(
                weights.astype(jnp.bfloat16), kv_past, preferred_element_type=jnp.float32
            )
        osend[i] = (value / total).astype(jnp.bfloat16)

        @pl.when(s != i)
        def _():
            o_copy(i).start()

        @pl.when(s == i)
        def _():
            obuf[i] = osend[i]

    w_gather.relay()
    for d in range(1, sp):
        j = s ^ d
        remote(obuf.at[j], obuf.at[j], o_send.at[0], o_recv.at[j], j, t).wait_recv()
    for r in range(g):
        part = pl.ds(r * piece, piece)
        if hpd == 1:
            attbuf[t, part, :] = obuf[r][:, :HD]
        else:
            low = lax.broadcasted_iota(jnp.int32, (piece, LANES), 1) < HD
            for p in range(hpd // 2):
                even = obuf[(2 * p) * g + r].astype(jnp.float32)
                odd = obuf[(2 * p + 1) * g + r].astype(jnp.float32)
                attbuf[t, part, p * LANES:(p + 1) * LANES] = jnp.where(low, even, odd).astype(jnp.bfloat16)
    a_gather = Gather(attbuf, ay_send, ap_send, a_recv, s, t, tp)
    a_gather.start()
    a_gather.relay()
    w_gather.finish()
    a_gather.finish()
    mixed = resid_ref[...].astype(jnp.float32)
    for a in range(tp):
        mixed = mixed + jnp.dot(attbuf[a], wbuf[a], preferred_element_type=jnp.float32)
    stream[...] = mixed
    square = jnp.mean(mixed * mixed, axis=1, keepdims=True)
    mine = pl.ds(pl.multiple_of(t * cols, cols), cols)
    here = stream[:, mine]
    stream_out[...] = here
    normed[...] = (here * lax.rsqrt(square + EPSILON) * gain_ref[:, mine]).astype(jnp.bfloat16)
    rows_out[...] = jnp.dot(
        pick_ref[...], normed[...], preferred_element_type=jnp.float32
    ).astype(jnp.bfloat16)
    for d in range(1, sp):
        q_copy(d).wait_send()
        kv_copy(d).wait_send()
    for i in range(sp):
        @pl.when(s != i)
        def _():
            o_copy(i).wait_send()
    w_gather.drain()
    a_gather.drain()


def expert_kernel(
    sp, tp, tile, rows_ref, wg_ref, wu_ref, wd_ref, hi_ref, lo_ref, stream_ref,
    out_ref,
    gath, wg, wu, wd, hid, psend, precv, ysend, yrecv, own, erows, ret,
    w_sem, x_send, x_recv, gy_send, gp_send, g_recv,
    ps_send, ps_recv, ys_send, ys_recv, r_send, r_recv,
):
    s, t = lax.axis_index("sp"), lax.axis_index("tp")
    ny = tp // 2
    half = sp // 2
    cap, cols = rows_ref.shape[1], rows_ref.shape[2]
    height = half * cap
    units = hid.shape[1]
    loads = [
        pltpu.make_async_copy(src, dst, w_sem.at[i])
        for i, (src, dst) in enumerate(((wg_ref, wg), (wu_ref, wu), (wd_ref, wd)))
    ]
    own_rows = pltpu.make_async_copy(rows_ref.at[0], gath.at[0, t], w_sem.at[3])
    own_rows.start()
    greet(sp, tp, s, t)

    def x_copy(d):
        return remote(rows_ref.at[d], gath.at[d, t], x_send.at[d], x_recv.at[d], s ^ offset_of(d, sp), t)

    for d in range(1, sp):
        x_copy(d).start()
    for load in loads:
        load.start()

    def gather_of(d):
        return Gather(gath.at[d], gy_send.at[d], gp_send.at[d], g_recv.at[d], s, t, tp)

    def forward(d):
        x_copy(d).wait_recv()
        gather_of(d).start()

    own_rows.wait()
    gather_of(0).start()
    for d in range(1, half):
        forward(d)
        gather_of(d - 1).relay()
    gather_of(half - 1).relay()
    for d in range(half):
        gather_of(d).finish()
    loads[0].wait()
    loads[1].wait()
    tiles = units // tile
    per_tile = half // tiles

    def gate_up(group, n):
        at = pl.ds(pl.multiple_of(n * tile, tile), tile)
        gate = jnp.zeros((height, tile), jnp.float32)
        up = jnp.zeros((height, tile), jnp.float32)
        for a in range(tp):
            x = gath[group * half:(group + 1) * half, a].reshape(height, cols)
            part = slice(a * cols, (a + 1) * cols)
            gate = gate + jnp.dot(x, wg[part, at], preferred_element_type=jnp.float32)
            up = up + jnp.dot(x, wu[part, at], preferred_element_type=jnp.float32)
        hid[:, at] = (gate / (1.0 + jnp.exp(-gate)) * up).astype(jnp.bfloat16)

    def first_tile(n, carry):
        for j in range(per_tile):
            d = half + n * per_tile + j
            if j:
                gather_of(d - 1).relay()
            else:
                @pl.when(n > 0)
                def _():
                    gather_of(d - 1).relay()
            forward(d)
        gate_up(0, n)
        return carry

    def second_tile(n, carry):
        gate_up(1, n)
        return carry

    def ps_copy(group, k):
        return remote(
            psend.at[group, k], precv.at[group, k], ps_send.at[group, k], ps_recv.at[group, k], s, t ^ 1
        )

    def ys_copy(group, k):
        return remote(
            ysend.at[group, k], yrecv.at[group, k], ys_send.at[group, k], ys_recv.at[group, k], s, t ^ (2 * k)
        )

    def r_copy(d):
        group, at = d // half, d % half
        return remote(erows.at[group, at], ret.at[d], r_send.at[d], r_recv.at[d], s ^ offset_of(d, sp), t)

    def down(group):
        def block(b):
            return jnp.dot(
                hid[...], wd[:, pl.ds(pl.multiple_of(b * cols, cols), cols)],
                preferred_element_type=jnp.float32,
            )

        order = list(range(1, ny)) + [0]
        for k in order:
            psend[group, k] = block(t ^ (2 * k + 1)).astype(jnp.bfloat16)
            ps_copy(group, k).start()
        for k in order:
            total = block(t ^ (2 * k))
            ps_copy(group, k).wait_recv()
            total = total + precv[group, k].astype(jnp.float32)
            if k:
                ysend[group, k] = total.astype(jnp.bfloat16)
                ys_copy(group, k).start()
            else:
                own[group] = total

    def give_back(group):
        total = own[group]
        for k in range(1, ny):
            ys_copy(group, k).wait_recv()
            total = total + yrecv[group, k].astype(jnp.float32)
        erows[group] = total.astype(jnp.bfloat16).reshape(half, cap, cols)
        for at in reversed(range(half)):
            d = group * half + at
            if d:
                r_copy(d).start()
            else:
                ret[0] = erows[0, 0]

    lax.fori_loop(0, tiles, first_tile, 0)
    gather_of(sp - 1).relay()
    loads[2].wait()
    down(0)
    for d in range(half, sp):
        gather_of(d).finish()
    lax.fori_loop(0, tiles, second_tile, 0)
    give_back(0)
    down(1)
    give_back(1)
    for d in range(1, sp):
        r_copy(d).wait_recv()
    back = ret[...].reshape(sp * cap, cols)
    combined = jnp.dot(hi_ref[...], back, preferred_element_type=jnp.float32)
    combined = combined + jnp.dot(lo_ref[...], back, preferred_element_type=jnp.float32)
    out_ref[...] = (stream_ref[...] + combined).astype(jnp.bfloat16)
    for d in range(1, sp):
        x_copy(d).wait_send()
        r_copy(d).wait_send()
    for d in range(sp):
        gather_of(d).drain()
    for group in range(2):
        for k in range(ny):
            ps_copy(group, k).wait_send()
            if k:
                ys_copy(group, k).wait_send()


def local(
    queries, keys, values, cum_gate, out_weight, resid, norm_gain, routes, route_weight,
    gate_weight, up_weight, down_weight,
):
    rows = queries.shape[0]
    hpd = queries.shape[1] // HD
    sp, tp = lax.axis_size("sp"), lax.axis_size("tp")
    s = lax.axis_index("sp")
    width = resid.shape[1]
    cols = width // tp
    g = sp // hpd
    piece = rows // g
    bf16, f32 = jnp.bfloat16, jnp.float32
    dma = pltpu.SemaphoreType.DMA

    def heads(x):
        return x.reshape(rows, hpd, HD).transpose(1, 0, 2)

    def packed(even_low, high):
        swap = (jnp.arange(hpd) % 2 == 0)[:, None, None]
        one = jnp.concatenate([even_low, high], axis=-1)
        two = jnp.concatenate([high, even_low], axis=-1)
        return jnp.where(swap, one, two)

    kv = packed(heads(values), heads(keys))
    scaled = queries * jnp.asarray(HD ** -0.5, bf16)
    q = packed(jnp.zeros((hpd, rows, HD), bf16), heads(scaled)).reshape(sp, piece, LANES)
    head_gate = lax.dynamic_slice_in_dim(cum_gate, s // g, 1, 0)
    cq = lax.dynamic_slice_in_dim(head_gate.reshape(sp, g, piece), s % g, 1, 1).reshape(sp, piece, 1)

    cap = 5 * rows // (2 * sp)
    slots = -(-cap // 16) * 16
    experts = offset_of(jnp.arange(sp, dtype=jnp.int32), sp) ^ s
    named = routes[:, :, None] == experts[None, None, :]
    count = jnp.sum(named.astype(bf16), axis=1)
    before = (jnp.arange(rows)[:, None] > jnp.arange(rows)[None, :]).astype(bf16)
    rank = jnp.dot(before, count, preferred_element_type=f32).astype(jnp.int32)
    at_rank = rank[:, :, None] == jnp.arange(slots, dtype=jnp.int32)[None, None, :]
    taken = at_rank & (count[:, :, None] > 0)
    weight = jnp.sum(jnp.where(named, route_weight[:, :, None], 0.0), axis=1)
    pick = taken.astype(bf16).transpose(1, 2, 0).reshape(sp * slots, rows)
    high = lax.reduce_precision(weight, 8, 7)
    low = weight - high
    hi = jnp.where(taken, high[:, :, None], 0.0).astype(bf16).reshape(rows, sp * slots)
    lo = jnp.where(taken, low[:, :, None], 0.0).astype(bf16).reshape(rows, sp * slots)

    vmem = pl.BlockSpec(memory_space=pltpu.VMEM)
    anywhere = pl.BlockSpec(memory_space=pl.ANY)
    ny = tp // 2
    stream_cols, outgoing = pl.pallas_call(
        functools.partial(attend_kernel, sp, tp, hpd),
        out_shape=(
            jax.ShapeDtypeStruct((rows, cols), f32),
            jax.ShapeDtypeStruct((sp * slots, cols), bf16),
        ),
        in_specs=[vmem] * 4 + [anywhere] + [vmem] * 3,
        out_specs=(vmem, vmem),
        scratch_shapes=[
            pltpu.VMEM((sp, piece, LANES), bf16),
            pltpu.VMEM((sp, rows, LANES), bf16),
            pltpu.VMEM((sp, piece, LANES), bf16),
            pltpu.VMEM((sp, piece, LANES), bf16),
            pltpu.VMEM((tp, hpd * HD, width), bf16),
            pltpu.VMEM((tp, rows, hpd * HD), bf16),
            pltpu.VMEM((rows, width), f32),
            pltpu.VMEM((rows, cols), bf16),
            dma((sp,)), dma((sp,)), dma((sp,)), dma((sp,)), dma((sp,)), dma((sp,)), dma((3,)),
            dma((ny,)), dma((ny,)), dma((tp,)), dma((ny,)), dma((ny,)), dma((tp,)),
        ],
        compiler_params=pltpu.CompilerParams(
            collective_id=0, has_side_effects=True, vmem_limit_bytes=VMEM_BYTES
        ),
        name="attend",
    )(q, kv, cq, head_gate, out_weight, resid, norm_gain[None, :], pick)

    units = gate_weight.shape[2]
    tile = min(256, units)
    half = sp // 2
    height = half * slots
    return pl.pallas_call(
        functools.partial(expert_kernel, sp, tp, tile),
        out_shape=jax.ShapeDtypeStruct((rows, cols), bf16),
        in_specs=[vmem] + [anywhere] * 3 + [vmem] * 3,
        out_specs=vmem,
        scratch_shapes=[
            pltpu.VMEM((sp, tp, slots, cols), bf16),
            pltpu.VMEM((width, units), bf16),
            pltpu.VMEM((width, units), bf16),
            pltpu.VMEM((units, width), bf16),
            pltpu.VMEM((height, units), bf16),
            pltpu.VMEM((2, ny, height, cols), bf16),
            pltpu.VMEM((2, ny, height, cols), bf16),
            pltpu.VMEM((2, ny, height, cols), bf16),
            pltpu.VMEM((2, ny, height, cols), bf16),
            pltpu.VMEM((2, height, cols), f32),
            pltpu.VMEM((2, half, slots, cols), bf16),
            pltpu.VMEM((sp, slots, cols), bf16),
            dma((4,)), dma((sp,)), dma((sp,)), dma((sp, ny)), dma((sp, ny)), dma((sp, tp)),
            dma((2, ny)), dma((2, ny)), dma((2, ny)), dma((2, ny)), dma((sp,)), dma((sp,)),
        ],
        compiler_params=pltpu.CompilerParams(
            collective_id=1, has_side_effects=True, vmem_limit_bytes=VMEM_BYTES
        ),
        name="experts",
    )(
        outgoing.reshape(sp, slots, cols), gate_weight[0], up_weight[0], down_weight[0], hi, lo, stream_cols
    )


def solution(mesh):
    return jax.shard_map(
        local,
        mesh=mesh,
        in_specs=(
            P("sp", "tp"), P("sp", "tp"), P("sp", "tp"), P("tp", None), P("tp", None), P("sp", None),
            P(), P("sp", None), P("sp", None), P("sp", None, "tp"), P("sp", None, "tp"), P("sp", "tp", None),
        ),
        out_specs=P("sp", "tp"),
        check_vma=False,
    )
```

profile of v0, /device:TPU:0, one launch (start us, length us, event | category | flops | bytes accessed | tf_op | source)
XLA Modules:
  0.0 120.3 jit_solution(4050062185110006149)
XLA Ops:
  0.0 0.0 copy-start
  0.0 0.8 copy-done
  0.8 0.0 copy-start.1
  0.8 1.1 copy.36.cq_ref
  1.9 0.8 fusion.3
  2.6 0.2 convolution_convert_fusion
  2.8 0.1 eq.72
  2.9 0.9 fusion.1.pick_ref
  3.8 1.0 copy.30
  4.9 0.2 copy.31
  5.0 1.0 copy.32
  6.0 0.0 copy-start.2
  6.1 0.0 copy-start.3
  6.1 0.2 copy.33
  6.2 1.0 copy.34
  7.3 0.2 copy.35
  7.5 1.2 %maximum_select_fusion = (bf16[4,256,128]{2,1,0:T(8,128)(2,1)}, bf16[4,256,128]{2,1,0:T(8,128)(2,1)}) fusion(bf16[4,256,64]{2,1,0:T(8,128)(2,1)S(1)} %bitcast.38, bf16[4,256,64]{2,1,0:T(8,128)(2,1)S(1)} %bitcast.37, pred[4]{0:T(512)(128)(4,1)S(1)} %fusion.7, bf16[4,256,64]{2,1,0:T(8,128)(2,1)S(1)} %bitcast.36), kind=kLoop, calls=%fused_computation.7 | loop fusion | flops 1310720 | bytes 917508 | tf_op jit(solution)/shard_map/jit(_where)/select_n | solution.py:380
  8.7 0.0 copy-done.1
  8.7 39.2 %attend.1 = (f32[256,512]{1,0:T(8,128)}, bf16[640,512]{1,0:T(8,128)(2,1)}) custom-call(bf16[8,128,128]{2,1,0:T(8,128)(2,1)} %bitcast.39, bf16[4,256,128]{2,1,0:T(8,128)(2,1)} %get-tuple-element.13.kv_ref, f32[8,128,1]{2,1,0:T(8,128)} %copy.36.cq_ref, f32[1,2048]{1,0:T(1,128)} %copy-done.1, bf16[256,2048]{1,0:T(8,128)(2,1)} %w_ref.1, ...), custom_call_target="tpu_custom_call" | custom-call | tf_op jit(solution)/shard_map/attend/pallas_call | solution.py:407
  47.9 0.2 copy.37
  48.2 0.3 copy.38
  48.5 0.0 copy-done.2
  48.5 0.0 copy-done.3
  48.5 0.1 fusion.2
  48.6 0.2 copy.40
  48.8 1.0 select_convert_fusion
  49.8 0.2 copy.39
  50.0 0.8 select_convert_fusion.1.hi_ref
  50.8 67.8 %experts.1 = bf16[256,512]{1,0:T(8,128)(2,1)} custom-call(bf16[8,80,512]{2,1,0:T(8,128)(2,1)} %bitcast.40, bf16[2048,1024]{1,0:T(8,128)(2,1)} %bitcast.30, bf16[2048,1024]{1,0:T(8,128)(2,1)} %bitcast.31, bf16[1024,2048]{1,0:T(8,128)(2,1)} %bitcast.32, bf16[256,640]{1,0:T(8,128)(2,1)} %select_convert_fusion.1.hi_ref, ...), custom_call_target="tpu_custom_call" | custom-call | tf_op jit(solution)/shard_map/experts/pallas_call | solution.py:437
  118.7 1.7 %copy.42 = bf16[256,512]{1,0:T(8,128)(2,1)} copy(bf16[256,512]{1,0:T(8,128)(2,1)} %experts.1) | data formatting | bytes 524288
  (13 shorter events, 0.3 us)
Async XLA Ops:
  0.0 0.8 copy-start
  0.8 7.9 %copy-start.1 = (f32[1,2048]{1,0:T(1,128)}, f32[1,2048]{1,0:T(1,128)S(1)}, u32[]{:S(2)}) copy-start(f32[1,2048]{1,0:T(1,128)S(1)} %constant_dynamic-slice_fusion.1.ck_ref) | copy-start | bytes 24580
  6.0 42.5 %copy-start.2 = (s32[256,2]{0,1:T(2,128)S(1)}, s32[256,2]{0,1:T(2,128)}, u32[]{:S(2)}) copy-start(s32[256,2]{0,1:T(2,128)} %param.19) | copy-start | bytes 6148
  6.1 42.5 %copy-start.3 = (f32[256,2]{0,1:T(2,128)S(1)}, f32[256,2]{0,1:T(2,128)}, u32[]{:S(2)}) copy-start(f32[256,2]{0,1:T(2,128)} %param.20) | copy-start | bytes 6148
where the time goes:
time: 121 us; the launch traced here: 120 us
  Pallas kernels  107 us (88%)
  local copies, waits for them, and re-layouts  8.23 us (7%)
  other arithmetic  4.8 us (4%)
    pallas_call x1, Pallas kernels, local(): pl.pallas_call(functools.partial(expert_kernel, sp, tp, tile), out_shape=...  67.8 us
    pallas_call x1, Pallas kernels, local(): pl.pallas_call(functools.partial(attend_kernel, sp, tp, hpd), out_shape=(...  39.2 us
    unnamed x12, local copies, waits for them, and re-layouts  5.46 us

commit v1 on v0

--- a/solution.py
+++ b/solution.py
@@ -211,148 +211,163 @@
 ):
     s, t = lax.axis_index("sp"), lax.axis_index("tp")
     ny = tp // 2
-    half = sp // 2
-    cap, cols = rows_ref.shape[1], rows_ref.shape[2]
-    height = half * cap
+    slots, cols = rows_ref.shape[1], rows_ref.shape[2]
     units = hid.shape[1]
+    f32, bf16 = jnp.float32, jnp.bfloat16
     loads = [
         pltpu.make_async_copy(src, dst, w_sem.at[i])
         for i, (src, dst) in enumerate(((wg_ref, wg), (wu_ref, wu), (wd_ref, wd)))
     ]
-    own_rows = pltpu.make_async_copy(rows_ref.at[0], gath.at[0, t], w_sem.at[3])
+
+    def window(a):
+        return pl.ds(pl.multiple_of(a * cols, cols), cols)
+
+    own_rows = pltpu.make_async_copy(rows_ref.at[0], gath.at[0, :, window(t)], w_sem.at[3])
     own_rows.start()
     greet(sp, tp, s, t)
 
     def x_copy(d):
-        return remote(rows_ref.at[d], gath.at[d, t], x_send.at[d], x_recv.at[d], s ^ offset_of(d, sp), t)
+        return remote(
+            rows_ref.at[d], gath.at[d, :, window(t)], x_send.at[d], x_recv.at[d], s ^ offset_of(d, sp), t
+        )
 
     for d in range(1, sp):
         x_copy(d).start()
     for load in loads:
         load.start()
 
-    def gather_of(d):
-        return Gather(gath.at[d], gy_send.at[d], gp_send.at[d], g_recv.at[d], s, t, tp)
+    def y_copy(d, k):
+        at = gath.at[d, :, window(t)]
+        return remote(at, at, gy_send.at[d, k], g_recv.at[d, t], s, t ^ (2 * k))
+
+    def p_copy(d, k):
+        a = t ^ (2 * k)
+        at = gath.at[d, :, window(a)]
+        return remote(at, at, gp_send.at[d, k], g_recv.at[d, a], s, t ^ 1)
+
+    def arrival(d, a):
+        at = gath.at[d, :, window(a)]
+        return remote(at, at, gp_send.at[d, 0], g_recv.at[d, a], s, t ^ 1)
+
+    def spread(d):
+        for k in range(1, ny):
+            y_copy(d, k).start()
+        p_copy(d, 0).start()
 
     def forward(d):
         x_copy(d).wait_recv()
-        gather_of(d).start()
-
-    own_rows.wait()
-    gather_of(0).start()
-    for d in range(1, half):
-        forward(d)
-        gather_of(d - 1).relay()
-    gather_of(half - 1).relay()
-    for d in range(half):
-        gather_of(d).finish()
-    loads[0].wait()
-    loads[1].wait()
-    tiles = units // tile
-    per_tile = half // tiles
-
-    def gate_up(group, n):
-        at = pl.ds(pl.multiple_of(n * tile, tile), tile)
-        gate = jnp.zeros((height, tile), jnp.float32)
-        up = jnp.zeros((height, tile), jnp.float32)
-        for a in range(tp):
-            x = gath[group * half:(group + 1) * half, a].reshape(height, cols)
-            part = slice(a * cols, (a + 1) * cols)
-            gate = gate + jnp.dot(x, wg[part, at], preferred_element_type=jnp.float32)
-            up = up + jnp.dot(x, wu[part, at], preferred_element_type=jnp.float32)
-        hid[:, at] = (gate / (1.0 + jnp.exp(-gate)) * up).astype(jnp.bfloat16)
-
-    def first_tile(n, carry):
-        for j in range(per_tile):
-            d = half + n * per_tile + j
-            if j:
-                gather_of(d - 1).relay()
-            else:
-                @pl.when(n > 0)
-                def _():
-                    gather_of(d - 1).relay()
-            forward(d)
-        gate_up(0, n)
-        return carry
-
-    def second_tile(n, carry):
-        gate_up(1, n)
-        return carry
-
-    def ps_copy(group, k):
-        return remote(
-            psend.at[group, k], precv.at[group, k], ps_send.at[group, k], ps_recv.at[group, k], s, t ^ 1
-        )
-
-    def ys_copy(group, k):
-        return remote(
-            ysend.at[group, k], yrecv.at[group, k], ys_send.at[group, k], ys_recv.at[group, k], s, t ^ (2 * k)
-        )
+        spread(d)
+
+    def relay(d):
+        for k in range(1, ny):
+            arrival(d, t ^ (2 * k)).wait_recv()
+            p_copy(d, k).start()
+
+    def finish(d):
+        for k in range(ny):
+            arrival(d, t ^ (2 * k + 1)).wait_recv()
+
+    def ps_copy(d, k):
+        return remote(psend.at[d, k], precv.at[d, k], ps_send.at[d, k], ps_recv.at[d, k], s, t ^ 1)
+
+    def ys_copy(d, k):
+        return remote(ysend.at[d, k], yrecv.at[d, k], ys_send.at[d, k], ys_recv.at[d, k], s, t ^ (2 * k))
 
     def r_copy(d):
-        group, at = d // half, d % half
-        return remote(erows.at[group, at], ret.at[d], r_send.at[d], r_recv.at[d], s ^ offset_of(d, sp), t)
-
-    def down(group):
+        return remote(erows.at[d], ret.at[d], r_send.at[d], r_recv.at[d], s ^ offset_of(d, sp), t)
+
+    def gate_up(d):
+        x = gath[d]
+        for n in range(units // tile):
+            at = slice(n * tile, (n + 1) * tile)
+            gate = jnp.dot(x, wg[:, at], preferred_element_type=f32)
+            up = jnp.dot(x, wu[:, at], preferred_element_type=f32)
+            hid[:, at] = (gate / (1.0 + jnp.exp(-gate)) * up).astype(bf16)
+
+    order = list(range(1, ny)) + [0]
+
+    def down(d):
         def block(b):
-            return jnp.dot(
-                hid[...], wd[:, pl.ds(pl.multiple_of(b * cols, cols), cols)],
-                preferred_element_type=jnp.float32,
-            )
-
-        order = list(range(1, ny)) + [0]
+            return jnp.dot(hid[...], wd[:, window(b)], preferred_element_type=f32)
+
         for k in order:
-            psend[group, k] = block(t ^ (2 * k + 1)).astype(jnp.bfloat16)
-            ps_copy(group, k).start()
+            psend[d, k] = block(t ^ (2 * k + 1)).astype(bf16)
+            ps_copy(d, k).start()
         for k in order:
             total = block(t ^ (2 * k))
-            ps_copy(group, k).wait_recv()
-            total = total + precv[group, k].astype(jnp.float32)
+            ps_copy(d, k).wait_recv()
+            total = total + precv[d, k].astype(f32)
             if k:
-                ysend[group, k] = total.astype(jnp.bfloat16)
-                ys_copy(group, k).start()
+                ysend[d, k] = total.astype(bf16)
+                ys_copy(d, k).start()
             else:
-                own[group] = total
-
-    def give_back(group):
-        total = own[group]
+                own[d] = total
+
+    def give_back(d):
+        total = own[d]
         for k in range(1, ny):
-            ys_copy(group, k).wait_recv()
-            total = total + yrecv[group, k].astype(jnp.float32)
-        erows[group] = total.astype(jnp.bfloat16).reshape(half, cap, cols)
-        for at in reversed(range(half)):
-            d = group * half + at
-            if d:
-                r_copy(d).start()
-            else:
-                ret[0] = erows[0, 0]
-
-    lax.fori_loop(0, tiles, first_tile, 0)
-    gather_of(sp - 1).relay()
-    loads[2].wait()
-    down(0)
-    for d in range(half, sp):
-        gather_of(d).finish()
-    lax.fori_loop(0, tiles, second_tile, 0)
-    give_back(0)
-    down(1)
-    give_back(1)
-    for d in range(1, sp):
-        r_copy(d).wait_recv()
-    back = ret[...].reshape(sp * cap, cols)
-    combined = jnp.dot(hi_ref[...], back, preferred_element_type=jnp.float32)
-    combined = combined + jnp.dot(lo_ref[...], back, preferred_element_type=jnp.float32)
-    out_ref[...] = (stream_ref[...] + combined).astype(jnp.bfloat16)
-    for d in range(1, sp):
-        x_copy(d).wait_send()
-        r_copy(d).wait_send()
+            ys_copy(d, k).wait_recv()
+            total = total + yrecv[d, k].astype(f32)
+        erows[d] = total.astype(bf16)
+
+    own_rows.wait()
+    spread(0)
+    forward(1)
+    relay(0)
+    for load in loads:
+        load.wait()
+
+    def step(n, carry):
+        @pl.when(n + 2 < sp)
+        def _():
+            forward(n + 2)
+
+        @pl.when(n + 1 < sp)
+        def _():
+            relay(n + 1)
+
+        finish(n)
+        gate_up(n)
+        down(n)
+
+        @pl.when(n > 0)
+        def _():
+            give_back(n - 1)
+
+            @pl.when(n > 1)
+            def _():
+                r_copy(n - 1).start()
+
+        return carry
+
+    lax.fori_loop(0, sp, step, 0)
+    give_back(sp - 1)
+    r_copy(sp - 1).start()
+    combined = stream_ref[...]
     for d in range(sp):
-        gather_of(d).drain()
-    for group in range(2):
+        if d:
+            r_copy(d).wait_recv()
+        back = ret[d] if d else erows[0]
+        part = slice(d * slots, (d + 1) * slots)
+        combined = combined + jnp.dot(hi_ref[:, part], back, preferred_element_type=f32)
+        combined = combined + jnp.dot(lo_ref[:, part], back, preferred_element_type=f32)
+    out_ref[...] = combined.astype(bf16)
+
+    def drain(d, carry):
+        @pl.when(d > 0)
+        def _():
+            x_copy(d).wait_send()
+            r_copy(d).wait_send()
+
         for k in range(ny):
-            ps_copy(group, k).wait_send()
+            p_copy(d, k).wait_send()
+            ps_copy(d, k).wait_send()
             if k:
-                ys_copy(group, k).wait_send()
+                y_copy(d, k).wait_send()
+                ys_copy(d, k).wait_send()
+        return carry
+
+    lax.fori_loop(0, sp, drain, 0)
 
 
 def local(
@@ -432,28 +447,26 @@
 
     units = gate_weight.shape[2]
     tile = min(256, units)
-    half = sp // 2
-    height = half * slots
     return pl.pallas_call(
         functools.partial(expert_kernel, sp, tp, tile),
         out_shape=jax.ShapeDtypeStruct((rows, cols), bf16),
         in_specs=[vmem] + [anywhere] * 3 + [vmem] * 3,
         out_specs=vmem,
         scratch_shapes=[
-            pltpu.VMEM((sp, tp, slots, cols), bf16),
+            pltpu.VMEM((sp, slots, width), bf16),
             pltpu.VMEM((width, units), bf16),
             pltpu.VMEM((width, units), bf16),
             pltpu.VMEM((units, width), bf16),
-            pltpu.VMEM((height, units), bf16),
-            pltpu.VMEM((2, ny, height, cols), bf16),
-            pltpu.VMEM((2, ny, height, cols), bf16),
-            pltpu.VMEM((2, ny, height, cols), bf16),
-            pltpu.VMEM((2, ny, height, cols), bf16),
-            pltpu.VMEM((2, height, cols), f32),
-            pltpu.VMEM((2, half, slots, cols), bf16),
+            pltpu.VMEM((slots, units), bf16),
+            pltpu.VMEM((sp, ny, slots, cols), bf16),
+            pltpu.VMEM((sp, ny, slots, cols), bf16),
+            pltpu.VMEM((sp, ny, slots, cols), bf16),
+            pltpu.VMEM((sp, ny, slots, cols), bf16),
+            pltpu.VMEM((sp, slots, cols), f32),
+            pltpu.VMEM((sp, slots, cols), bf16),
             pltpu.VMEM((sp, slots, cols), bf16),
             dma((4,)), dma((sp,)), dma((sp,)), dma((sp, ny)), dma((sp, ny)), dma((sp, tp)),
-            dma((2, ny)), dma((2, ny)), dma((2, ny)), dma((2, ny)), dma((sp,)), dma((sp,)),
+            dma((sp, ny)), dma((sp, ny)), dma((sp, ny)), dma((sp, ny)), dma((sp,)), dma((sp,)),
         ],
         compiler_params=pltpu.CompilerParams(
             collective_id=1, has_side_effects=True, vmem_limit_bytes=VMEM_BYTES

time: 121 us -> 110 us (0.909)
  Pallas kernels: 107 us -> 96.4 us
    pallas_call x1, Pallas kernels: 67.8 us -> 57.2 us  [local(): pl.pallas_call(functools.partial(expert_kernel, sp, tp, tile), out_shape=...]
where the time goes in v1:
time: 110 us
  Pallas kernels  96.4 us (88%)
  local copies, waits for them, and re-layouts  8.23 us (7%)
  other arithmetic  4.8 us (4%)
    pallas_call x1, Pallas kernels, local(): pl.pallas_call(functools.partial(expert_kernel, sp, tp, tile), out_shape=...  57.2 us
    pallas_call x1, Pallas kernels, local(): pl.pallas_call(functools.partial(attend_kernel, sp, tp, hpd), out_shape=(...  39.2 us
    unnamed x12, local copies, waits for them, and re-layouts  5.46 us

profile of v1, /device:TPU:0, one launch (start us, length us, event | category | flops | bytes accessed | tf_op | source)
XLA Modules:
  0.0 109.7 jit_solution(17445921061804897119)
XLA Ops:
  0.0 0.0 copy-start
  0.0 0.8 copy-done
  0.8 0.0 copy-start.1
  0.8 1.1 copy.36.cq_ref
  1.9 0.8 fusion.3
  2.6 0.2 convolution_convert_fusion
  2.8 0.1 eq.72
  2.9 0.9 fusion.1.pick_ref
  3.8 1.0 copy.30
  4.9 0.2 copy.31
  5.0 1.0 copy.32
  6.0 0.0 copy-start.2
  6.1 0.0 copy-start.3
  6.1 0.2 copy.33
  6.2 1.0 copy.34
  7.3 0.2 copy.35
  7.5 1.2 %maximum_select_fusion = (bf16[4,256,128]{2,1,0:T(8,128)(2,1)}, bf16[4,256,128]{2,1,0:T(8,128)(2,1)}) fusion(bf16[4,256,64]{2,1,0:T(8,128)(2,1)S(1)} %bitcast.38, bf16[4,256,64]{2,1,0:T(8,128)(2,1)S(1)} %bitcast.37, pred[4]{0:T(512)(128)(4,1)S(1)} %fusion.7, bf16[4,256,64]{2,1,0:T(8,128)(2,1)S(1)} %bitcast.36), kind=kLoop, calls=%fused_computation.7 | loop fusion | flops 1310720 | bytes 917508 | tf_op jit(solution)/shard_map/jit(_where)/select_n | solution.py:395
  8.7 0.0 copy-done.1
  8.7 39.2 %attend.1 = (f32[256,512]{1,0:T(8,128)}, bf16[640,512]{1,0:T(8,128)(2,1)}) custom-call(bf16[8,128,128]{2,1,0:T(8,128)(2,1)} %bitcast.39, bf16[4,256,128]{2,1,0:T(8,128)(2,1)} %get-tuple-element.13.kv_ref, f32[8,128,1]{2,1,0:T(8,128)} %copy.36.cq_ref, f32[1,2048]{1,0:T(1,128)} %copy-done.1, bf16[256,2048]{1,0:T(8,128)(2,1)} %w_ref.1, ...), custom_call_target="tpu_custom_call" | custom-call | tf_op jit(solution)/shard_map/attend/pallas_call | solution.py:422
  47.9 0.2 copy.37
  48.2 0.3 copy.38
  48.5 0.0 copy-done.2
  48.5 0.0 copy-done.3
  48.5 0.1 fusion.2
  48.6 0.2 copy.40
  48.8 1.0 select_convert_fusion
  49.8 0.2 copy.39
  50.0 0.8 select_convert_fusion.1.hi_ref
  50.8 57.2 %experts.1 = bf16[256,512]{1,0:T(8,128)(2,1)} custom-call(bf16[8,80,512]{2,1,0:T(8,128)(2,1)} %bitcast.40, bf16[2048,1024]{1,0:T(8,128)(2,1)} %bitcast.30, bf16[2048,1024]{1,0:T(8,128)(2,1)} %bitcast.31, bf16[1024,2048]{1,0:T(8,128)(2,1)} %bitcast.32, bf16[256,640]{1,0:T(8,128)(2,1)} %select_convert_fusion.1.hi_ref, ...), custom_call_target="tpu_custom_call" | custom-call | tf_op jit(solution)/shard_map/experts/pallas_call | solution.py:450
  108.1 1.7 %copy.42 = bf16[256,512]{1,0:T(8,128)(2,1)} copy(bf16[256,512]{1,0:T(8,128)(2,1)} %experts.1) | data formatting | bytes 524288
  (13 shorter events, 0.3 us)
Async XLA Ops:
  0.0 0.8 copy-start
  0.8 7.9 %copy-start.1 = (f32[1,2048]{1,0:T(1,128)}, f32[1,2048]{1,0:T(1,128)S(1)}, u32[]{:S(2)}) copy-start(f32[1,2048]{1,0:T(1,128)S(1)} %constant_dynamic-slice_fusion.1.ck_ref) | copy-start | bytes 24580
  6.0 42.5 %copy-start.2 = (s32[256,2]{0,1:T(2,128)S(1)}, s32[256,2]{0,1:T(2,128)}, u32[]{:S(2)}) copy-start(s32[256,2]{0,1:T(2,128)} %param.19) | copy-start | bytes 6148
  6.1 42.5 %copy-start.3 = (f32[256,2]{0,1:T(2,128)S(1)}, f32[256,2]{0,1:T(2,128)}, u32[]{:S(2)}) copy-start(f32[256,2]{0,1:T(2,128)} %param.20) | copy-start | bytes 6148

commit v2 on v1

v2 whole, which is shorter than its diff:
```python
import functools

import jax
import jax.numpy as jnp
from jax import lax
from jax.experimental import pallas as pl
from jax.experimental.pallas import tpu as pltpu
from jax.sharding import PartitionSpec as P

HD = 64
LANES = 128
EPSILON = 1e-06
MESH = pl.DeviceIdType.MESH
VMEM_BYTES = 60 * 1024 * 1024
CONTRACT_LAST = (((1,), (1,)), ((), ()))


def remote(src, dst, send_sem, recv_sem, s, t):
    return pltpu.make_async_remote_copy(
        src_ref=src,
        dst_ref=dst,
        send_sem=send_sem,
        recv_sem=recv_sem,
        device_id=(s, t),
        device_id_type=MESH,
    )


def offset_of(d, sp):
    half = sp // 2
    low, top = (d // 2) % 2, d // half
    return d - 2 * low - half * top + half * low + 2 * top


def units_of(sp):
    if sp == 8:
        return [(0, 2), (2, 1), (3, 1), (4, 2), (6, 1), (7, 1)]
    return [(d, 2) for d in range(0, sp, 2)]


def layer_kernel(
    sp, tp, hpd, slots, tile,
    q_ref, k_ref, v_ref, cum_ref, gain_ref, routes_ref, share_ref,
    w_ref, resid_ref, wg_ref, wu_ref, wd_ref,
    out_ref,
    kvs, kvbuf, qs, qbuf, osend, obuf, ckb, cqb, wbuf, attbuf, resbuf, stream, sums, pick, share,
    rows, gath, wg, wu, wd, hid, psend, precv, part, ysend, yrecv, erows, ret,
    local_sem, load_sem, kv_send, kv_relay, kv_recv, q_send, q_recv, o_send, o_recv,
    w_send, w_recv, ay_send, ap_send, a_recv, n_send, n_recv,
    x_send, x_recv, gy_send, gp_send, g_recv, ps_send, ps_recv, ys_send, ys_recv, r_send, r_recv,
):
    f32, bf16 = jnp.float32, jnp.bfloat16
    s, t = lax.axis_index("sp"), lax.axis_index("tp")
    ny = tp // 2
    g = sp // hpd
    tokens = q_ref.shape[0]
    piece = tokens // g
    packed = qs.shape[1] < piece
    short = qs.shape[1]
    width = gath.shape[2]
    cols = width // tp
    units = hid.shape[1]

    def window(a):
        return pl.ds(pl.multiple_of(a * cols, cols), cols)

    own_w = pltpu.make_async_copy(w_ref.at[:, window(t)], wbuf.at[t], local_sem.at[0])
    own_resid = pltpu.make_async_copy(resid_ref.at[:, window(t)], resbuf, local_sem.at[1])
    loads = [
        pltpu.make_async_copy(src.at[0], dst, load_sem.at[i])
        for i, (src, dst) in enumerate(((wg_ref, wg), (wu_ref, wu), (wd_ref, wd)))
    ]

    barrier = pltpu.get_barrier_semaphore()
    for d in range(1, sp):
        pl.semaphore_signal(barrier, inc=1, device_id=(s ^ d, t), device_id_type=MESH)
    for a in range(1, tp):
        pl.semaphore_signal(barrier, inc=1, device_id=(s, t ^ a), device_id_type=MESH)
    own_w.start()
    own_resid.start()

    def swap(x):
        return jnp.concatenate([x[:, HD:], x[:, :HD]], axis=1)

    def low_lanes(n):
        return lax.broadcasted_iota(jnp.int32, (n, LANES), 1) < HD

    if hpd == 1:
        kvs[0] = jnp.concatenate([v_ref[...], k_ref[...]], axis=1)
        q = q_ref[...].astype(f32) * HD ** -0.5
        q = jnp.concatenate([jnp.zeros_like(q), q], axis=1).astype(bf16)
        for j in range(sp):
            qs[j] = q[j * piece:(j + 1) * piece]
    else:
        low = low_lanes(tokens)
        for p in range(hpd // 2):
            pair = slice(p * LANES, (p + 1) * LANES)
            k = swap(k_ref[:, pair].astype(f32))
            v = v_ref[:, pair].astype(f32)
            kvs[2 * p] = jnp.where(low, v, k).astype(bf16)
            kvs[2 * p + 1] = jnp.where(low, k, v).astype(bf16)
            q = q_ref[:, pair].astype(f32) * HD ** -0.5
            turned = swap(q)
            for odd in range(2):
                for r in range(g):
                    at = r * piece
                    front = turned[at:at + short]
                    back = q[at + short:at + piece] if packed else jnp.zeros_like(front)
                    keys_low = low_lanes(short)
                    both = jnp.where(keys_low, front, back) if odd else jnp.where(keys_low, back, front)
                    qs[(2 * p + odd) * g + r] = both.astype(bf16)
    pl.semaphore_wait(barrier, sp + tp - 2)

    def kv_copy(d):
        dst = s ^ d
        return remote(kvs.at[dst // g], kvbuf.at[s], kv_send.at[d], kv_recv.at[s], dst, t)

    def kv_pass(d):
        i = s ^ d
        src = kvbuf.at[i] if d else kvs.at[s // g]
        return remote(src, kvbuf.at[i], kv_relay.at[d], kv_recv.at[i], s ^ 1, t)

    def kv_arrival(i):
        return remote(kvbuf.at[i], kvbuf.at[i], kv_relay.at[0], kv_recv.at[i], s ^ 1, t)

    def q_copy(d):
        dst = s ^ d
        return remote(qs.at[dst], qbuf.at[s], q_send.at[d], q_recv.at[s], dst, t)

    def w_copy(a):
        return remote(w_ref.at[:, window(t ^ a)], wbuf.at[t], w_send.at[a], w_recv.at[t], s, t ^ a)

    for d in range(sp - 2, 1, -2):
        kv_copy(d).start()
    kv_pass(0).start()
    for d in range(sp - 1, 0, -1):
        q_copy(d).start()
    for a in range(1, tp):
        w_copy(a).start()
    for load in loads:
        load.start()
    kvbuf[s] = kvs[s // g]
    qbuf[s] = qs[s]

    head = s // g
    first = lax.rem(s, g) * piece
    qpos = first + lax.broadcasted_iota(jnp.int32, (piece, tokens), 0)
    kpos = lax.broadcasted_iota(jnp.int32, (piece, tokens), 1)
    ckb[...] = cum_ref[pl.ds(head, 1), :]
    for i in range(sp):
        here = ckb[:, i * tokens:(i + 1) * tokens]
        cqb[i] = jnp.sum(jnp.where(kpos == qpos, here, 0.0), axis=1, keepdims=True)
    experts = offset_of(lax.broadcasted_iota(jnp.int32, (sp, tokens), 0), sp) ^ s
    chosen = [routes_ref[k:k + 1, :] == experts for k in range(2)]
    named = jnp.where(chosen[0] | chosen[1], 1.0, 0.0)
    weight = sum(jnp.where(chosen[k], share_ref[k:k + 1, :], 0.0) for k in range(2))
    high = weight.astype(bf16).astype(f32)
    parts = (high, weight - high)
    across = lax.broadcasted_iota(jnp.int32, (tokens, tokens), 1)
    along = lax.broadcasted_iota(jnp.int32, (tokens, tokens), 0)
    before = jnp.where(along < across, 1.0, 0.0).astype(bf16)
    rank = jnp.dot(named.astype(bf16), before, preferred_element_type=f32)
    rank = jnp.where(named > 0.0, rank, -1.0)
    slot = lax.broadcasted_iota(jnp.int32, (slots, tokens), 0).astype(f32)
    shares = ([], [])
    for d in range(sp):
        taken = slot == rank[d:d + 1, :]
        pick[d * slots:(d + 1) * slots, :] = jnp.where(taken, 1.0, 0.0).astype(bf16)
        for n in range(2):
            shares[n].append(jnp.where(taken, parts[n][d:d + 1, :], 0.0))
    for n in range(2):
        share[n] = jnp.concatenate(shares[n], axis=0).T.astype(bf16)

    for d in range(2, sp, 2):
        kv_arrival(s ^ d).wait_recv()
        kv_pass(d).start()

    def o_copy(i):
        return remote(osend.at[i], obuf.at[s], o_send.at[i], o_recv.at[s], i, t)

    half = lax.broadcasted_iota(jnp.int32, (short, LANES), 1) // HD
    key_lanes = (half + lax.rem(head, 2)) == 1
    for i in range(sp):
        @pl.when(s != i)
        def _():
            remote(qbuf.at[i], qbuf.at[i], q_send.at[0], q_recv.at[i], s ^ 1, t).wait_recv()

        @pl.when((s != i) & (lax.rem(s + i, 2) == 1))
        def _():
            kv_arrival(i).wait_recv()

        q = qbuf[i]
        if packed:
            q = q.astype(f32)
            q = jnp.concatenate(
                [jnp.where(key_lanes, q, 0.0), jnp.where(key_lanes, swap(q), 0.0)], axis=0
            ).astype(bf16)
        cq = cqb[i]
        kv_here = kvbuf[i]
        diag = lax.dot_general(q, kv_here, CONTRACT_LAST, preferred_element_type=f32)
        diag = diag + cq - ckb[:, i * tokens:(i + 1) * tokens]
        diag = jnp.where(kpos <= qpos, diag, -jnp.inf)
        best = jnp.max(diag, axis=1, keepdims=True)
        if i:
            kv_past = kvbuf[0:i].reshape(i * tokens, LANES)
            past = lax.dot_general(q, kv_past, CONTRACT_LAST, preferred_element_type=f32)
            past = past + cq - ckb[:, :i * tokens]
            best = jnp.maximum(best, jnp.max(past, axis=1, keepdims=True))
        weights = jnp.exp(diag - best)
        total = jnp.sum(weights, axis=1, keepdims=True)
        value = jnp.dot(weights.astype(bf16), kv_here, preferred_element_type=f32)
        if i:
            weights = jnp.exp(past - best)
            total = total + jnp.sum(weights, axis=1, keepdims=True)
            value = value + jnp.dot(weights.astype(bf16), kv_past, preferred_element_type=f32)
        value = value / total
        if packed:
            value = jnp.where(key_lanes, swap(value[short:]), value[:short])
        osend[i] = value.astype(bf16)

        @pl.when(s != i)
        def _():
            o_copy(i).start()

        @pl.when(s == i)
        def _():
            obuf[i] = osend[i]

    for d in range(1, sp):
        j = s ^ d
        remote(obuf.at[j], obuf.at[j], o_send.at[0], o_recv.at[j], j, t).wait_recv()
    low = low_lanes(short)
    for r in range(g):
        at = r * piece
        if hpd == 1:
            attbuf[t, at:at + piece, :] = obuf[r][:, :HD]
        else:
            for p in range(hpd // 2):
                pair = slice(p * LANES, (p + 1) * LANES)
                even = obuf[(2 * p) * g + r].astype(f32)
                odd = obuf[(2 * p + 1) * g + r].astype(f32)
                attbuf[t, at:at + short, pair] = jnp.where(low, even, odd).astype(bf16)
                if packed:
                    attbuf[t, at + short:at + piece, pair] = swap(jnp.where(low, odd, even)).astype(bf16)

    def ay_copy(k):
        at = attbuf.at[t]
        return remote(at, at, ay_send.at[k], a_recv.at[t], s, t ^ (2 * k))

    def ap_copy(k):
        a = t ^ (2 * k)
        at = attbuf.at[a]
        return remote(at, at, ap_send.at[k], a_recv.at[a], s, t ^ 1)

    def a_arrival(a):
        at = attbuf.at[a]
        return remote(at, at, ap_send.at[0], a_recv.at[a], s, t ^ 1)

    for k in range(1, ny):
        ay_copy(k).start()
    ap_copy(0).start()
    for k in range(1, ny):
        a_arrival(t ^ (2 * k)).wait_recv()
        ap_copy(k).start()
    own_w.wait()
    own_resid.wait()
    for a in range(1, tp):
        remote(wbuf.at[t ^ a], wbuf.at[t ^ a], w_send.at[0], w_recv.at[t ^ a], s, t ^ 1).wait_recv()
    for k in range(ny):
        a_arrival(t ^ (2 * k + 1)).wait_recv()
    mixed = resbuf[...].astype(f32)
    for a in range(tp):
        mixed = mixed + jnp.dot(attbuf[a], wbuf[a], preferred_element_type=f32)
    stream[...] = mixed
    square = jnp.sum(mixed * mixed, axis=1, keepdims=True)
    sums[t] = jnp.sum(jnp.where(along == across, square, 0.0), axis=0, keepdims=True)

    def n_copy(a):
        return remote(sums.at[t], sums.at[t], n_send.at[a], n_recv.at[t], s, t ^ a)

    for a in range(1, tp):
        n_copy(a).start()
    for a in range(1, tp):
        at = sums.at[t ^ a]
        remote(at, at, n_send.at[0], n_recv.at[t ^ a], s, t ^ 1).wait_recv()
    square = sums[0]
    for a in range(1, tp):
        square = square + sums[a]
    scale = lax.rsqrt(square / width + EPSILON)
    scale = jnp.sum(jnp.where(along == across, scale, 0.0), axis=1, keepdims=True)
    normed = (stream[...] * scale * gain_ref[:, window(t)]).astype(bf16)

    def x_copy(d):
        return remote(
            rows.at[d], gath.at[d, :, window(t)], x_send.at[d], x_recv.at[d], s ^ offset_of(d, sp), t
        )

    def y_copy(d, k):
        at = gath.at[d, :, window(t)]
        return remote(at, at, gy_send.at[d, k], g_recv.at[d, t], s, t ^ (2 * k))

    def p_copy(d, k):
        a = t ^ (2 * k)
        at = gath.at[d, :, window(a)]
        return remote(at, at, gp_send.at[d, k], g_recv.at[d, a], s, t ^ 1)

    def arrival(d, a):
        at = gath.at[d, :, window(a)]
        return remote(at, at, gp_send.at[d, 0], g_recv.at[d, a], s, t ^ 1)

    def forward(d):
        if d:
            x_copy(d).wait_recv()
        for k in range(1, ny):
            y_copy(d, k).start()
        p_copy(d, 0).start()

    def relay(d):
        for k in range(1, ny):
            arrival(d, t ^ (2 * k)).wait_recv()
            p_copy(d, k).start()

    def finish(d):
        for k in range(ny):
            arrival(d, t ^ (2 * k + 1)).wait_recv()

    def send(d, n):
        out = jnp.dot(pick[d * slots:(d + n) * slots, :], normed, preferred_element_type=f32).astype(bf16)
        for j in range(n):
            block = out[j * slots:(j + 1) * slots]
            if d + j:
                rows[d + j] = block
                x_copy(d + j).start()
            else:
                gath[0, :, window(t)] = block
                forward(0)

    pairs = [d for d in range(0, sp, 2)]
    for d in pairs[1:2] + pairs[:1] + pairs[2:]:
        send(d, 2)

    def ps_copy(d, k):
        return remote(psend.at[d, k], precv.at[d, k], ps_send.at[d, k], ps_recv.at[d, k], s, t ^ 1)

    def ys_copy(d, k):
        return remote(ysend.at[d, k], yrecv.at[d, k], ys_send.at[d, k], ys_recv.at[d, k], s, t ^ (2 * k))

    def r_copy(d):
        return remote(erows.at[d], ret.at[d], r_send.at[d], r_recv.at[d], s ^ offset_of(d, sp), t)

    def gate_up(d, n, tiles):
        x = gath[d:d + n].reshape(n * slots, width)
        for j in tiles:
            at = slice(j * tile, (j + 1) * tile)
            gate = jnp.dot(x, wg[:, at], preferred_element_type=f32)
            up = jnp.dot(x, wu[:, at], preferred_element_type=f32)
            hid[:n * slots, at] = (gate / (1.0 + jnp.exp(-gate)) * up).astype(bf16)

    order = list(range(1, ny)) + [0]

    def block(n, b):
        return jnp.dot(hid[:n * slots, :], wd[:, window(b)], preferred_element_type=f32)

    def down_pair(d, n):
        for k in order:
            out = block(n, t ^ (2 * k + 1)).astype(bf16)
            for j in range(n):
                psend[d + j, k] = out[j * slots:(j + 1) * slots]
                ps_copy(d + j, k).start()

    def down_own(d, n):
        for k in order:
            out = block(n, t ^ (2 * k))
            for j in range(n):
                part[d + j, k] = out[j * slots:(j + 1) * slots]

    def add_pair(d, n):
        for k in order:
            for j in range(n):
                ps_copy(d + j, k).wait_recv()
                total = part[d + j, k] + precv[d + j, k].astype(f32)
                if k:
                    ysend[d + j, k] = total.astype(bf16)
                    ys_copy(d + j, k).start()
                else:
                    part[d + j, k] = total

    def give_back(d, n):
        for j in range(d, d + n):
            total = part[j, 0]
            for k in range(1, ny):
                ys_copy(j, k).wait_recv()
                total = total + yrecv[j, k].astype(f32)
            erows[j] = total.astype(bf16)
            if j:
                r_copy(j).start()

    actions = [functools.partial(forward, 1)]

    def advance(limit):
        nonlocal done
        for action in actions[done:limit]:
            action()
        done = max(done, min(limit, len(actions)))

    for d in range(sp):
        if 0 < d < sp - 1:
            actions.append(functools.partial(forward, d + 1))
        actions.append(functools.partial(relay, d))
    done = 0
    work = units_of(sp)
    tiles = list(range(units // tile))
    cut = len(tiles) // 2
    loaded = False
    for n, unit in enumerate(work):
        last = unit[0] + unit[1] - 1
        advance(min(2 * last + 2, len(actions)))
        for d in range(unit[0], last + 1):
            finish(d)
        if not loaded:
            for load in loads:
                load.wait()
            loaded = True
        gate_up(*unit, tiles[:cut])
        if n:
            add_pair(*work[n - 1])
        gate_up(*unit, tiles[cut:])
        advance(done + 1)
        down_pair(*unit)
        if n > 1:
            give_back(*work[n - 2])
        down_own(*unit)
        advance(done + 1)
    add_pair(*work[-1])
    give_back(*work[-2])
    give_back(*work[-1])

    ret[0] = erows[0]
    for d in range(1, sp):
        r_copy(d).wait_recv()
    back = ret[...].reshape(sp * slots, cols)
    combined = jnp.dot(share[0], back, preferred_element_type=f32)
    combined = combined + jnp.dot(share[1], back, preferred_element_type=f32)
    combined = stream[...] + combined
    out_ref[...] = combined.astype(bf16)

    for d in range(1, sp):
        q_copy(d).wait_send()
        if d % 2 == 0:
            kv_copy(d).wait_send()
            kv_pass(d).wait_send()
    kv_pass(0).wait_send()
    for i in range(sp):
        @pl.when(s != i)
        def _():
            o_copy(i).wait_send()
    for a in range(1, tp):
        w_copy(a).wait_send()
        n_copy(a).wait_send()
    for k in range(ny):
        ap_copy(k).wait_send()
        if k:
            ay_copy(k).wait_send()

    def drain(d, carry):
        @pl.when(d > 0)
        def _():
            x_copy(d).wait_send()
            r_copy(d).wait_send()

        for k in range(ny):
            p_copy(d, k).wait_send()
            ps_copy(d, k).wait_send()
            if k:
                y_copy(d, k).wait_send()
                ys_copy(d, k).wait_send()
        return carry

    lax.fori_loop(0, sp, drain, 0)


def local(
    queries, keys, values, cum_gate, out_weight, resid, norm_gain, routes, route_weight,
    gate_weight, up_weight, down_weight,
):
    tokens = queries.shape[0]
    hpd = queries.shape[1] // HD
    sp, tp = lax.axis_size("sp"), lax.axis_size("tp")
    width = resid.shape[1]
    cols = width // tp
    units = gate_weight.shape[2]
    tile = min(256, units)
    piece = tokens // (sp // hpd)
    short = piece // 2 if hpd > 1 and piece % 32 == 0 else piece
    cap = 5 * tokens // (2 * sp)
    slots = -(-cap // 16) * 16
    ny = tp // 2
    bf16, f32 = jnp.bfloat16, jnp.float32
    dma = pltpu.SemaphoreType.DMA

    def vm(*shape, dtype=bf16):
        return pltpu.VMEM(shape, dtype)

    vmem = pl.BlockSpec(memory_space=pltpu.VMEM)
    anywhere = pl.BlockSpec(memory_space=pl.ANY)
    return pl.pallas_call(
        functools.partial(layer_kernel, sp, tp, hpd, slots, tile),
        out_shape=jax.ShapeDtypeStruct((tokens, cols), bf16),
        in_specs=[vmem] * 7 + [anywhere] * 5,
        out_specs=vmem,
        scratch_shapes=[
            vm(hpd, tokens, LANES), vm(sp, tokens, LANES),
            vm(sp, short, LANES), vm(sp, short, LANES), vm(sp, short, LANES), vm(sp, short, LANES),
            vm(1, sp * tokens, dtype=f32), vm(sp, piece, 1, dtype=f32),
            vm(tp, hpd * HD, cols), vm(tp, tokens, hpd * HD), vm(tokens, cols),
            vm(tokens, cols, dtype=f32), vm(tp, 1, tokens, dtype=f32),
            vm(sp * slots, tokens), vm(2, tokens, sp * slots),
            vm(sp, slots, cols), vm(sp, slots, width),
            vm(width, units), vm(width, units), vm(units, width), vm(2 * slots, units),
            vm(sp, ny, slots, cols), vm(sp, ny, slots, cols), vm(sp, ny, slots, cols, dtype=f32),
            vm(sp, ny, slots, cols), vm(sp, ny, slots, cols), vm(sp, slots, cols), vm(sp, slots, cols),
            dma((2,)), dma((3,)), dma((sp,)), dma((sp,)), dma((sp,)), dma((sp,)), dma((sp,)),
            dma((sp,)), dma((sp,)),
            dma((tp,)), dma((tp,)), dma((ny,)), dma((ny,)), dma((tp,)), dma((tp,)), dma((tp,)),
            dma((sp,)), dma((sp,)), dma((sp, ny)), dma((sp, ny)), dma((sp, tp)),
            dma((sp, ny)), dma((sp, ny)), dma((sp, ny)), dma((sp, ny)), dma((sp,)), dma((sp,)),
        ],
        compiler_params=pltpu.CompilerParams(
            collective_id=0, has_side_effects=True, vmem_limit_bytes=VMEM_BYTES
        ),
        name="layer",
    )(
        queries, keys, values, cum_gate, norm_gain[None, :], routes.T, route_weight.T,
        out_weight, resid, gate_weight, up_weight, down_weight,
    )


def solution(mesh):
    return jax.shard_map(
        local,
        mesh=mesh,
        in_specs=(
            P("sp", "tp"), P("sp", "tp"), P("sp", "tp"), P("tp", None), P("tp", None), P("sp", None),
            P(), P("sp", None), P("sp", None), P("sp", None, "tp"), P("sp", None, "tp"), P("sp", "tp", None),
        ),
        out_specs=P("sp", "tp"),
        check_vma=False,
    )
```

time: 110 us -> 86.6 us (0.79)
  Pallas kernels: 96.4 us -> 84.7 us
  local copies, waits for them, and re-layouts: 8.23 us -> 1.67 us
  other arithmetic: 4.8 us -> 0 us
    pallas_call x2 -> x1, Pallas kernels: 96.4 us -> 84.7 us  [local(): pl.pallas_call(functools.partial(layer_kernel, sp, tp, hpd, slots, tile),...]
    unnamed x12 -> x1, local copies, waits for them, and re-layouts: 5.46 us -> 1.67 us
    convert_element_type x3 -> x0, other arithmetic: 2.68 us -> none  [the longest x1 0.95 us: local(): jnp.where(taken, low[:, :, None], 0.0).astype(bf16)]
    reshape x4 -> x0, local copies, waits for them, and re-layouts: 1.58 us -> none  [the longest x1 1.07 us: local(): lax.dynamic_slice_in_dim(head_gate.reshape(sp, g, piece), s % g, 1, 1)]
    select_n x1 -> x0, other arithmetic: 1.24 us -> none  [packed(): return jnp.where(swap, one, two)]
where the time goes in v2:
time: 86.6 us; the launch traced here: 86.4 us
  Pallas kernels  84.7 us (98%)
  local copies, waits for them, and re-layouts  1.67 us (2%)
    pallas_call x1, Pallas kernels, local(): pl.pallas_call(functools.partial(layer_kernel, sp, tp, hpd, slots, tile),...  84.7 us

profile of v2, /device:TPU:0, one launch (start us, length us, event | category | flops | bytes accessed | tf_op | source)
XLA Modules:
  0.0 86.4 jit_solution(14548594289168975490)
XLA Ops:
  0.0 84.7 %layer.1 = bf16[256,512]{1,0:T(8,128)(2,1)} custom-call(bf16[256,256]{1,0:T(8,128)(2,1)} %q_ref.1, bf16[256,256]{1,0:T(8,128)(2,1)} %k_ref.1, bf16[256,256]{1,0:T(8,128)(2,1)} %v_ref.1, f32[4,2048]{1,0:T(4,128)} %cum_ref.1, f32[1,2048]{1,0:T(1,128)} %bitcast.3, s32[2,256]{1,0:T(2,128)} %bitcast.4, f32[2,256]{1,0:T(2,128)} %bitcast.5, ...), custom_call_target="tpu_custom_call" | custom-call | tf_op jit(solution)/shard_map/layer/pallas_call | solution.py:506
  84.8 1.7 %copy.14 = bf16[256,512]{1,0:T(8,128)(2,1)} copy(bf16[256,512]{1,0:T(8,128)(2,1)} %layer.1) | data formatting | bytes 524288

commit v3 on v2

--- a/solution.py
+++ b/solution.py
@@ -26,24 +26,12 @@
     )
 
 
-def offset_of(d, sp):
-    half = sp // 2
-    low, top = (d // 2) % 2, d // half
-    return d - 2 * low - half * top + half * low + 2 * top
-
-
-def units_of(sp):
-    if sp == 8:
-        return [(0, 2), (2, 1), (3, 1), (4, 2), (6, 1), (7, 1)]
-    return [(d, 2) for d in range(0, sp, 2)]
-
-
 def layer_kernel(
     sp, tp, hpd, slots, tile,
     q_ref, k_ref, v_ref, cum_ref, gain_ref, routes_ref, share_ref,
     w_ref, resid_ref, wg_ref, wu_ref, wd_ref,
     out_ref,
-    kvs, kvbuf, qs, qbuf, osend, obuf, ckb, cqb, wbuf, attbuf, resbuf, stream, sums, pick, share,
+    kvs, kvbuf, qs, qbuf, osend, obuf, ckb, cqb, wsrc, wbuf, attbuf, resbuf, stream, sums, pick, share,
     rows, gath, wg, wu, wd, hid, psend, precv, part, ysend, yrecv, erows, ret,
     local_sem, load_sem, kv_send, kv_relay, kv_recv, q_send, q_recv, o_send, o_recv,
     w_send, w_recv, ay_send, ap_send, a_recv, n_send, n_recv,
@@ -65,6 +53,7 @@
         return pl.ds(pl.multiple_of(a * cols, cols), cols)
 
     own_w = pltpu.make_async_copy(w_ref.at[:, window(t)], wbuf.at[t], local_sem.at[0])
+    all_w = pltpu.make_async_copy(w_ref, wsrc, local_sem.at[2])
     own_resid = pltpu.make_async_copy(resid_ref.at[:, window(t)], resbuf, local_sem.at[1])
     loads = [
         pltpu.make_async_copy(src.at[0], dst, load_sem.at[i])
@@ -76,6 +65,7 @@
         pl.semaphore_signal(barrier, inc=1, device_id=(s ^ d, t), device_id_type=MESH)
     for a in range(1, tp):
         pl.semaphore_signal(barrier, inc=1, device_id=(s, t ^ a), device_id_type=MESH)
+    all_w.start()
     own_w.start()
     own_resid.start()
 
@@ -128,13 +118,14 @@
         return remote(qs.at[dst], qbuf.at[s], q_send.at[d], q_recv.at[s], dst, t)
 
     def w_copy(a):
-        return remote(w_ref.at[:, window(t ^ a)], wbuf.at[t], w_send.at[a], w_recv.at[t], s, t ^ a)
+        return remote(wsrc.at[:, window(t ^ a)], wbuf.at[t], w_send.at[a], w_recv.at[t], s, t ^ a)
 
     for d in range(sp - 2, 1, -2):
         kv_copy(d).start()
     kv_pass(0).start()
     for d in range(sp - 1, 0, -1):
         q_copy(d).start()
+    all_w.wait()
     for a in range(1, tp):
         w_copy(a).start()
     for load in loads:
@@ -150,7 +141,7 @@
     for i in range(sp):
         here = ckb[:, i * tokens:(i + 1) * tokens]
         cqb[i] = jnp.sum(jnp.where(kpos == qpos, here, 0.0), axis=1, keepdims=True)
-    experts = offset_of(lax.broadcasted_iota(jnp.int32, (sp, tokens), 0), sp) ^ s
+    experts = lax.broadcasted_iota(jnp.int32, (sp, tokens), 0) ^ s
     chosen = [routes_ref[k:k + 1, :] == experts for k in range(2)]
     named = jnp.where(chosen[0] | chosen[1], 1.0, 0.0)
     weight = sum(jnp.where(chosen[k], share_ref[k:k + 1, :], 0.0) for k in range(2))
@@ -163,7 +154,9 @@
     rank = jnp.where(named > 0.0, rank, -1.0)
     slot = lax.broadcasted_iota(jnp.int32, (slots, tokens), 0).astype(f32)
     shares = ([], [])
-    for d in range(sp):
+    plan = [0] + list(range(4, sp, 2)) + [2]
+    places = [d + j for d in plan for j in range(2)]
+    for d in places:
         taken = slot == rank[d:d + 1, :]
         pick[d * slots:(d + 1) * slots, :] = jnp.where(taken, 1.0, 0.0).astype(bf16)
         for n in range(2):
@@ -288,11 +281,11 @@
         square = square + sums[a]
     scale = lax.rsqrt(square / width + EPSILON)
     scale = jnp.sum(jnp.where(along == across, scale, 0.0), axis=1, keepdims=True)
-    normed = (stream[...] * scale * gain_ref[:, window(t)]).astype(bf16)
+    resbuf[...] = (stream[...] * scale * gain_ref[:, window(t)]).astype(bf16)
 
     def x_copy(d):
         return remote(
-            rows.at[d], gath.at[d, :, window(t)], x_send.at[d], x_recv.at[d], s ^ offset_of(d, sp), t
+            rows.at[d], gath.at[d, :, window(t)], x_send.at[d], x_recv.at[d], s ^ d, t
         )
 
     def y_copy(d, k):
@@ -325,7 +318,7 @@
             arrival(d, t ^ (2 * k + 1)).wait_recv()
 
     def send(d, n):
-        out = jnp.dot(pick[d * slots:(d + n) * slots, :], normed, preferred_element_type=f32).astype(bf16)
+        out = jnp.dot(pick[d * slots:(d + n) * slots, :], resbuf[...], preferred_element_type=f32).astype(bf16)
         for j in range(n):
             block = out[j * slots:(j + 1) * slots]
             if d + j:
@@ -335,9 +328,16 @@
                 gath[0, :, window(t)] = block
                 forward(0)
 
-    pairs = [d for d in range(0, sp, 2)]
-    for d in pairs[1:2] + pairs[:1] + pairs[2:]:
+    late = 3 * sp // 8 * 2
+    for d in range(0, late, 2):
         send(d, 2)
+    forward(1)
+    relay(0)
+    forward(2)
+    for d in range(late, sp, 2):
+        send(d, 2)
+    relay(1)
+    forward(3)
 
     def ps_copy(d, k):
         return remote(psend.at[d, k], precv.at[d, k], ps_send.at[d, k], ps_recv.at[d, k], s, t ^ 1)
@@ -345,8 +345,9 @@
     def ys_copy(d, k):
         return remote(ysend.at[d, k], yrecv.at[d, k], ys_send.at[d, k], ys_recv.at[d, k], s, t ^ (2 * k))
 
-    def r_copy(d):
-        return remote(erows.at[d], ret.at[d], r_send.at[d], r_recv.at[d], s ^ offset_of(d, sp), t)
+    def r_copy(d, place=0):
+        at = ret.at[pl.ds(place * slots, slots)]
+        return remote(erows.at[d], at, r_send.at[d], r_recv.at[d], s ^ d, t)
 
     def gate_up(d, n, tiles):
         x = gath[d:d + n].reshape(n * slots, width)
@@ -393,52 +394,42 @@
                 total = total + yrecv[j, k].astype(f32)
             erows[j] = total.astype(bf16)
             if j:
-                r_copy(j).start()
-
-    actions = [functools.partial(forward, 1)]
-
-    def advance(limit):
-        nonlocal done
-        for action in actions[done:limit]:
-            action()
-        done = max(done, min(limit, len(actions)))
-
-    for d in range(sp):
-        if 0 < d < sp - 1:
-            actions.append(functools.partial(forward, d + 1))
-        actions.append(functools.partial(relay, d))
-    done = 0
-    work = units_of(sp)
-    tiles = list(range(units // tile))
-    cut = len(tiles) // 2
-    loaded = False
-    for n, unit in enumerate(work):
-        last = unit[0] + unit[1] - 1
-        advance(min(2 * last + 2, len(actions)))
-        for d in range(unit[0], last + 1):
-            finish(d)
-        if not loaded:
+                r_copy(j, places.index(j)).start()
+
+    tiles = range(units // tile)
+    for n, d in enumerate(plan):
+        finish(d)
+        finish(d + 1)
+        if not n:
             for load in loads:
                 load.wait()
-            loaded = True
-        gate_up(*unit, tiles[:cut])
-        if n:
-            add_pair(*work[n - 1])
-        gate_up(*unit, tiles[cut:])
-        advance(done + 1)
-        down_pair(*unit)
+        gate_up(d, 2, tiles)
+        if not n:
+            forward(4)
+        down_pair(d, 2)
+        if not n:
+            forward(5)
+        down_own(d, 2)
         if n > 1:
-            give_back(*work[n - 2])
-        down_own(*unit)
-        advance(done + 1)
-    add_pair(*work[-1])
-    give_back(*work[-2])
-    give_back(*work[-1])
-
-    ret[0] = erows[0]
-    for d in range(1, sp):
-        r_copy(d).wait_recv()
-    back = ret[...].reshape(sp * slots, cols)
+            give_back(plan[n - 1], 2)
+        add_pair(d, 2)
+        if n == 1:
+            give_back(plan[0], 2)
+        if not n:
+            relay(2)
+            relay(3)
+        if n + 3 < len(plan):
+            forward(plan[n + 2])
+            forward(plan[n + 2] + 1)
+        if n + 2 < len(plan):
+            relay(plan[n + 1])
+            relay(plan[n + 1] + 1)
+    give_back(plan[-1], 2)
+
+    ret[:slots] = erows[0]
+    for n in range(1, sp):
+        r_copy(places[n], n).wait_recv()
+    back = ret[...]
     combined = jnp.dot(share[0], back, preferred_element_type=f32)
     combined = combined + jnp.dot(share[1], back, preferred_element_type=f32)
     combined = stream[...] + combined
@@ -512,14 +503,14 @@
             vm(hpd, tokens, LANES), vm(sp, tokens, LANES),
             vm(sp, short, LANES), vm(sp, short, LANES), vm(sp, short, LANES), vm(sp, short, LANES),
             vm(1, sp * tokens, dtype=f32), vm(sp, piece, 1, dtype=f32),
-            vm(tp, hpd * HD, cols), vm(tp, tokens, hpd * HD), vm(tokens, cols),
+            vm(hpd * HD, width), vm(tp, hpd * HD, cols), vm(tp, tokens, hpd * HD), vm(tokens, cols),
             vm(tokens, cols, dtype=f32), vm(tp, 1, tokens, dtype=f32),
             vm(sp * slots, tokens), vm(2, tokens, sp * slots),
             vm(sp, slots, cols), vm(sp, slots, width),
             vm(width, units), vm(width, units), vm(units, width), vm(2 * slots, units),
             vm(sp, ny, slots, cols), vm(sp, ny, slots, cols), vm(sp, ny, slots, cols, dtype=f32),
-            vm(sp, ny, slots, cols), vm(sp, ny, slots, cols), vm(sp, slots, cols), vm(sp, slots, cols),
-            dma((2,)), dma((3,)), dma((sp,)), dma((sp,)), dma((sp,)), dma((sp,)), dma((sp,)),
+            vm(sp, ny, slots, cols), vm(sp, ny, slots, cols), vm(sp, slots, cols), vm(sp * slots, cols),
+            dma((3,)), dma((3,)), dma((sp,)), dma((sp,)), dma((sp,)), dma((sp,)), dma((sp,)),
             dma((sp,)), dma((sp,)),
             dma((tp,)), dma((tp,)), dma((ny,)), dma((ny,)), dma((tp,)), dma((tp,)), dma((tp,)),
             dma((sp,)), dma((sp,)), dma((sp, ny)), dma((sp, ny)), dma((sp, tp)),

time: 86.6 us -> 83.3 us (0.962)
  Pallas kernels: 84.7 us -> 81.5 us
    pallas_call x1, Pallas kernels: 84.7 us -> 81.5 us  [local(): pl.pallas_call(functools.partial(layer_kernel, sp, tp, hpd, slots, tile),...]
where the time goes in v3:
time: 83.3 us; the launch traced here: 83.2 us
  Pallas kernels  81.5 us (98%)
  local copies, waits for them, and re-layouts  1.67 us (2%)
    pallas_call x1, Pallas kernels, local(): pl.pallas_call(functools.partial(layer_kernel, sp, tp, hpd, slots, tile),...  81.5 us
    unnamed x1, local copies, waits for them, and re-layouts  1.67 us

profile of v3, /device:TPU:0, one launch (start us, length us, event | category | flops | bytes accessed | tf_op | source)
XLA Modules:
  0.0 83.2 jit_solution(11344326167283695932)
XLA Ops:
  0.0 81.5 %layer.1 = bf16[256,512]{1,0:T(8,128)(2,1)} custom-call(bf16[256,256]{1,0:T(8,128)(2,1)} %q_ref.1, bf16[256,256]{1,0:T(8,128)(2,1)} %k_ref.1, bf16[256,256]{1,0:T(8,128)(2,1)} %v_ref.1, f32[4,2048]{1,0:T(4,128)} %cum_ref.1, f32[1,2048]{1,0:T(1,128)} %bitcast.3, s32[2,256]{1,0:T(2,128)} %bitcast.4, f32[2,256]{1,0:T(2,128)} %bitcast.5, ...), custom_call_target="tpu_custom_call" | custom-call | tf_op jit(solution)/shard_map/layer/pallas_call | solution.py:497
  81.5 1.7 %copy.14 = bf16[256,512]{1,0:T(8,128)(2,1)} copy(bf16[256,512]{1,0:T(8,128)(2,1)} %layer.1) | data formatting | bytes 524288

commit v4 on v3

--- a/solution.py
+++ b/solution.py
@@ -120,11 +120,9 @@
     def w_copy(a):
         return remote(wsrc.at[:, window(t ^ a)], wbuf.at[t], w_send.at[a], w_recv.at[t], s, t ^ a)
 
-    for d in range(sp - 2, 1, -2):
+    for d in range(2, sp, 2):
         kv_copy(d).start()
     kv_pass(0).start()
-    for d in range(sp - 1, 0, -1):
-        q_copy(d).start()
     all_w.wait()
     for a in range(1, tp):
         w_copy(a).start()
@@ -167,6 +165,9 @@
     for d in range(2, sp, 2):
         kv_arrival(s ^ d).wait_recv()
         kv_pass(d).start()
+        if d == 2:
+            for j in range(sp - 1, 0, -1):
+                q_copy(j).start()
 
     def o_copy(i):
         return remote(osend.at[i], obuf.at[s], o_send.at[i], o_recv.at[s], i, t)

time: 83.3 us -> 81.4 us (0.977)
  Pallas kernels: 81.5 us -> 79.5 us
    pallas_call x1, Pallas kernels: 81.5 us -> 79.5 us  [local(): pl.pallas_call(functools.partial(layer_kernel, sp, tp, hpd, slots, tile),...]
where the time goes in v4:
time: 81.4 us; the launch traced here: 81.2 us
  Pallas kernels  79.5 us (98%)
  local copies, waits for them, and re-layouts  1.67 us (2%)
    pallas_call x1, Pallas kernels, local(): pl.pallas_call(functools.partial(layer_kernel, sp, tp, hpd, slots, tile),...  79.5 us
    unnamed x1, local copies, waits for them, and re-layouts  1.67 us

profile of v4, /device:TPU:0, one launch (start us, length us, event | category | flops | bytes accessed | tf_op | source)
XLA Modules:
  0.0 81.2 jit_solution(16399860527388902992)
XLA Ops:
  0.0 79.5 %layer.1 = bf16[256,512]{1,0:T(8,128)(2,1)} custom-call(bf16[256,256]{1,0:T(8,128)(2,1)} %q_ref.1, bf16[256,256]{1,0:T(8,128)(2,1)} %k_ref.1, bf16[256,256]{1,0:T(8,128)(2,1)} %v_ref.1, f32[4,2048]{1,0:T(4,128)} %cum_ref.1, f32[1,2048]{1,0:T(1,128)} %bitcast.3, s32[2,256]{1,0:T(2,128)} %bitcast.4, f32[2,256]{1,0:T(2,128)} %bitcast.5, ...), custom_call_target="tpu_custom_call" | custom-call | tf_op jit(solution)/shard_map/layer/pallas_call | solution.py:498
  79.5 1.7 %copy.14 = bf16[256,512]{1,0:T(8,128)(2,1)} copy(bf16[256,512]{1,0:T(8,128)(2,1)} %layer.1) | data formatting | bytes 524288
